TPU v7x, 32 devices: a whole 2x2x4 slice. The times are simulated.
32 devices in a mesh: sp: 8 (over z, x), tp: 4 (over y, core).
Axes of the slice: x: 2, y: 2, z: 4, core: 2. Of those that a mesh axis runs over, the one named last changes fastest.
Arguments:
- residual: bfloat16 [1024, 2048], P('sp'), may hold values from -6 to 6
- queries: bfloat16 [1024, 2048], P('sp', 'tp'), may hold values from -6 to 6
- keys: bfloat16 [1024, 2048], P('sp', 'tp'), may hold values from -6 to 6
- values: bfloat16 [1024, 2048], P('sp', 'tp'), may hold values from -24 to 24
- stick_bias: bfloat16 [32, 1024], P('tp', 'sp'), may hold values from 2 to 13
- query_gain: float32 [64], replicated, may hold values from 0.1 to 1.9
- key_gain: float32 [64], replicated, may hold values from 0.1 to 1.9
- out_weight: bfloat16 [2048, 2048], P('tp'), may hold values from -0.25 to 0.25
- norm_gain: float32 [2048], replicated, may hold values from 0.1 to 1.9
- route_ids: int32 [1024, 2], P('sp'), may hold values from 0 to 7, all different within a row; in each aligned block of 128 rows (0 to 127, 128 to 255, ...) at most 40 rows name the same one
- route_weights: float32 [1024, 2], P('sp'), may hold values from 0.1 to 1
- gate_weight: bfloat16 [8, 2048, 2048], P('sp', None, 'tp'), may hold values from -3 to 3
- up_weight: bfloat16 [8, 2048, 2048], P('sp', None, 'tp'), may hold values from -3 to 3
- down_weight: bfloat16 [8, 2048, 2048], P('sp', 'tp'), may hold values from -0.125 to 0.125
Outputs:
- layer_out: bfloat16 [1024, 2048], P('sp', 'tp')
Inputs may be any that keep to these rules, and one draw needn't show every extreme that they name: `route_ids`: each row names 2 different experts. In every aligned block of 128 rows at most 40 rows name one expert, and in every draw some expert is named by exactly 40 rows of some block.
All inputs are finite; a program needn't handle non-finite values.
Results may differ from a plain program's by a relative error of at most 0.028.
Values may be sent and summed in bfloat16 or wider, within the bound.
A program may use at most 64 MiB of HBM per device.

v0:
```python
import math
import jax
import jax.numpy as jnp
from jax import lax
from jax.sharding import PartitionSpec as P

epsilon = 1e-06
clamp_limit = 7.0
swish_scale = 1.702


def head_normalize(packed, gain):
    values_f = packed.astype(jnp.float32).reshape(packed.shape[0], -1, gain.shape[0])
    scaled = (
        values_f * lax.rsqrt(jnp.mean(values_f * values_f, axis=-1, keepdims=True) + epsilon) * gain
    )
    return scaled.astype(jnp.bfloat16)


def activate(gate_pre, up_pre):
    gate_top = jnp.minimum(gate_pre, clamp_limit)
    up_clip = jnp.clip(up_pre, -clamp_limit, clamp_limit)
    return (up_clip + 1.0) * (gate_top * jax.nn.sigmoid(swish_scale * gate_top))


def slot_table(picked, expert_count, capacity):
    flat_ids = picked.reshape(-1)
    one_hot = (flat_ids[:, None] == jnp.arange(expert_count, dtype=jnp.int32)[None, :]).astype(
        jnp.int32
    )
    before = jnp.sum((jnp.cumsum(one_hot, axis=0) - one_hot) * one_hot, axis=1)
    return flat_ids * capacity + before


def key_block(state_pair, queries_n, keys_block, values_block, bias_block, first_key, query_pos):
    summed, log_carry = state_pair
    key_count = bias_block.shape[1]
    head_total = bias_block.shape[0]
    keys_heads = keys_block.reshape(key_count, head_total, -1)
    values_heads = values_block.reshape(key_count, head_total, -1)
    head_dim = keys_heads.shape[2]
    scores = jnp.einsum(
        "qhd,khd->hqk", queries_n, keys_heads, preferred_element_type=jnp.float32
    ) * head_dim ** (-0.5)
    scores = scores - bias_block.astype(jnp.float32)[:, None, :]
    key_pos = first_key + jnp.arange(key_count, dtype=jnp.int32)
    causal = ((key_pos[None, :] < query_pos[:, None]) & (key_pos[None, :] >= 0))[None]
    log_stay = jnp.where(causal, jax.nn.log_sigmoid(-scores), 0.0)
    later_sum = lax.cumsum(log_stay, axis=2, reverse=True) - log_stay
    weight = jnp.where(
        causal, jnp.exp(jax.nn.log_sigmoid(scores) + later_sum + log_carry[:, :, None]), 0.0
    )
    summed = summed + jnp.einsum(
        "hqk,khd->qhd",
        weight.astype(jnp.bfloat16),
        values_heads,
        preferred_element_type=jnp.float32,
    )
    return (summed, log_carry + jnp.sum(log_stay, axis=2))


def per_device(
    residual,
    queries,
    keys,
    values,
    stick_bias,
    query_gain,
    key_gain,
    out_weight,
    norm_gain,
    route_ids,
    route_weights,
    gate_weight,
    up_weight,
    down_weight,
):
    tok_rows = queries.shape[0]
    width_sp = lax.axis_size("sp")
    offset = lax.axis_index("sp") * tok_rows
    query_pos = offset + jnp.arange(tok_rows, dtype=jnp.int32)
    queries_n = head_normalize(queries, query_gain)
    keys_n = head_normalize(keys, key_gain).reshape(tok_rows, -1)
    head_total = stick_bias.shape[0]
    head_dim = query_gain.shape[0]
    state_pair = (
        jnp.zeros((tok_rows, head_total, head_dim), jnp.float32),
        jnp.zeros((head_total, tok_rows), jnp.float32),
    )
    all_keys, all_values, all_bias = (
        lax.all_gather(keys_n, "sp", axis=0, tiled=True),
        lax.all_gather(values, "sp", axis=0, tiled=True),
        lax.all_gather(stick_bias, "sp", axis=1, tiled=True),
    )
    key_total = all_keys.shape[0]
    block_len = math.gcd(key_total, 512)
    block_total = key_total // block_len

    def sweep_block(block_step, running):
        first_key = (block_total - 1 - block_step) * block_len
        return key_block(
            running,
            queries_n,
            lax.dynamic_slice_in_dim(all_keys, first_key, block_len, 0),
            lax.dynamic_slice_in_dim(all_values, first_key, block_len, 0),
            lax.dynamic_slice_in_dim(all_bias, first_key, block_len, 1),
            first_key,
            query_pos,
        )

    state_pair = lax.fori_loop(0, block_total, sweep_block, state_pair)
    attended = state_pair[0].reshape(tok_rows, head_total * head_dim).astype(jnp.bfloat16)
    partial_value = jnp.dot(attended, out_weight, preferred_element_type=jnp.float32)
    model_width = residual.shape[1]
    expert_count = width_sp * gate_weight.shape[0]
    pick_count = route_ids.shape[1]
    capacity = (5 * tok_rows * pick_count + 4 * expert_count - 1) // (4 * expert_count)
    slot_index = slot_table(route_ids, expert_count, capacity)
    assigned = slot_index.shape[0]
    source = (
        jnp.zeros((expert_count * capacity,), jnp.int32)
        .at[slot_index]
        .set(jnp.arange(assigned, dtype=jnp.int32) // pick_count)
    )
    filled = (
        jnp.zeros((expert_count * capacity,), jnp.bfloat16)
        .at[slot_index]
        .set(jnp.ones((assigned,), jnp.bfloat16))
    )
    gate_local = gate_weight[0]
    up_local = up_weight[0]
    down_local = down_weight[0]
    mixed_share = lax.psum_scatter(
        partial_value.astype(jnp.bfloat16), "tp", scatter_dimension=1, tiled=True
    ).astype(jnp.float32)
    own_width = mixed_share.shape[1]
    col_start = lax.axis_index("tp") * own_width
    own_res = lax.dynamic_slice_in_dim(residual, col_start, own_width, 1).astype(jnp.float32)
    own_cols = (own_res + mixed_share).astype(jnp.bfloat16).astype(jnp.float32)
    square_total = lax.psum(jnp.sum(own_cols * own_cols, axis=1), "tp")
    gain_cols = lax.dynamic_slice_in_dim(norm_gain, col_start, own_width, 0)
    normed_share = (
        own_cols * lax.rsqrt(square_total / model_width + epsilon)[:, None] * gain_cols
    ).astype(jnp.bfloat16)
    outgoing = (normed_share[source] * filled[:, None]).reshape(expert_count, capacity, -1)
    piece = lax.all_gather(
        lax.all_to_all(outgoing, "sp", split_axis=0, concat_axis=0, tiled=True),
        "tp",
        axis=2,
        tiled=True,
    )
    gate_pre = jnp.einsum("scd,df->scf", piece, gate_local, preferred_element_type=jnp.float32)
    up_pre = jnp.einsum("scd,df->scf", piece, up_local, preferred_element_type=jnp.float32)
    hidden = activate(gate_pre, up_pre).astype(jnp.bfloat16)
    share = jnp.einsum("scf,fd->scd", hidden, down_local, preferred_element_type=jnp.float32)
    returned = lax.psum_scatter(share.astype(jnp.bfloat16), "tp", scatter_dimension=2, tiled=True)
    arrived = lax.all_to_all(returned, "sp", split_axis=0, concat_axis=0, tiled=True)
    columns = arrived.shape[2]
    taken_rows = arrived.reshape(expert_count * capacity, columns)[slot_index]
    taken_rows = taken_rows.astype(jnp.float32).reshape(tok_rows, pick_count, columns)
    routed = jnp.sum(taken_rows * route_weights[:, :, None], axis=1)
    return (own_cols + routed).astype(jnp.bfloat16)


def solution(mesh):
    placed = (
        P("sp", None),
        P("sp", "tp"),
        P("sp", "tp"),
        P("sp", "tp"),
        P("tp", "sp"),
        P(),
        P(),
        P("tp", None),
        P(),
        P("sp", None),
        P("sp", None),
        P("sp", None, "tp"),
        P("sp", None, "tp"),
        P("sp", "tp", None),
    )
    return jax.shard_map(
        per_device, mesh=mesh, in_specs=placed, out_specs=P("sp", "tp"), check_vma=False
    )
```

profile of v0, /device:TPU:0, one launch (start us, length us, event | category | flops | bytes accessed | tf_op | source)
XLA Modules:
  0.0 249.5 jit_solution(2540238676448930279)
XLA Ops:
  6.5 1.2 copy.26
  7.8 0.7 mul.146
  8.4 0.1 mul.147
  8.5 0.8 fusion.52
  9.3 0.0 all-gather.6.cloned.1.call-update
  9.3 0.0 all-gather.4.cloned.1.call-start
  9.4 1.7 copy.25
  11.1 0.0 reduce-scatter.3.cloned.1.call-start
  11.1 1.0 copy.27
  12.1 0.8 copy.29
  12.9 0.1 eq.29
  13.1 0.6 reduce-window.24
  13.7 28.2 %all_gather.14 = bf16[8,1024]{1,0:T(8,128)(2,1)S(1)} all-gather(bf16[8,128]{1,0:T(8,128)(2,1)} %param.20), channel_id=1, replica_groups=mesh['sp'=8,'tp'=4] {'sp'}, dimensions={1}, use_global_device_ids=true | all-gather | bytes 18432 | tf_op jit(solution)/shard_map/all_gather | solution.py:93
  42.0 0.7 multiply_convert_fusion
  42.7 8.9 %all-gather.6.cloned.1.call-done = bf16[1024,512]{0,1:T(8,128)(2,1)} async-done(((bf16[128,512]{0,1:T(8,128)(2,1)}), bf16[1024,512]{0,1:T(8,128)(2,1)}) %all-gather.6.cloned.1.call-update) | async-done | bytes 1048592 | tf_op jit(solution)/shard_map/all_gather | solution.py:91
  51.6 40.3 %all-gather.4.cloned.1.call-done = bf16[1024,512]{0,1:T(8,128)(2,1)} async-done(((bf16[128,512]{0,1:T(8,128)(2,1)}), bf16[1024,512]{0,1:T(8,128)(2,1)}) %all-gather.4.cloned.1.call-update) | async-done | bytes 1048592 | tf_op jit(solution)/shard_map/all_gather | solution.py:92
  91.9 33.3 %while.16 = (s32[]{:T(128)}, f32[128,8,64]{0,2,1:T(8,128)S(1)}, f32[8,128]{1,0:T(8,128)S(1)}, bf16[1024,512]{0,1:T(8,128)(2,1)}, bf16[1024,512]{0,1:T(8,128)(2,1...) while((s32[]{:T(128)}, f32[128,8,64]{0,2,1:T(8,128)S(1)}, ...), condition=%wide.region_6.7_spmd.clone, body=%wide.region_2.6_spmd.clone.sunk | while | flops 219436672 | bytes 27240652 | solution.py:111
  91.9 1.3 constant_dynamic-slice_fusion.3
  93.2 0.2 compare_and_fusion.2
  93.4 3.0 %fusion.93 = (f32[8,128]{1,0:T(8,128)S(1)}, f32[8,128,512]{1,2,0:T(8,128)S(1)}, f32[8,512,128]{2,1,0:T(8,128)}) fusion(f32[8,512]{1,0:T(8,128)S(1)} %dynamic-slice_convert_fusion.2, pred[128,512]{0,1:T(8,128)(4,1)S(1)} %compare_and_fusion.2, bf16[512,8,64]{0,2,1:T(8,128)(2,1)S(1)} %bitcast.116, bf16[128,8,64]{0,2,1:T(8,128)(2,1)S(1)} %get-tuple-element.292), kind=kOutput, calls=%fused_computation.39.clone.1 | convolution fusion | flops 72875008 | bytes 4935680 | tf_op jit(solution)/shard_map/while/body/eval_jaxpr/qhd,khd->hqk/dot_general | solution.py:42
  96.4 5.0 %fusion.94 = f32[8,128,4,128]{1,0,3,2:T(8,128)S(1)} fusion(f32[8,128,4,128]{1,3,2,0:T(8,128)S(1)} %bitcast.114), kind=kOutput, calls=%fused_computation.23.clone.1 | output fusion | flops 66584576 | bytes 4194304 | tf_op jit(solution)/shard_map/reduce-window.6
  101.5 0.1 broadcast_add_fusion.2
  101.6 1.7 copy.38
  103.3 4.8 %fusion.97 = bf16[8,128,512]{1,2,0:T(8,128)(2,1)S(1)} fusion(f32[8,128,4,128]{1,3,2,0:T(8,128)} %copy.38, f32[8,512,128]{2,1,0:T(8,128)} %get-tuple-element.259, f32[8,128]{1,0:T(8,128)S(1)} %get-tuple-element.261, f32[8,512]{1,0:T(8,128)S(1)} %dynamic-slice_convert_fusion.2, pred[128,512]{0,1:T(8,128)(4,1)S(1)} %compare_and_fusion.2), kind=kLoop, calls=%fused_computation.12.clone.1 | loop fusion | flops 12058624 | bytes 5328896 | tf_op jit(solution)/shard_map/while/body/eval_jaxpr/convert_element_type | solution.py:55
  108.1 0.3 fusion.98
  108.5 1.3 constant_dynamic-slice_fusion.3
  109.8 0.2 compare_and_fusion.2
  110.1 3.0 %fusion.93 = (f32[8,128]{1,0:T(8,128)S(1)}, f32[8,128,512]{1,2,0:T(8,128)S(1)}, f32[8,512,128]{2,1,0:T(8,128)}) fusion(f32[8,512]{1,0:T(8,128)S(1)} %dynamic-slice_convert_fusion.2, pred[128,512]{0,1:T(8,128)(4,1)S(1)} %compare_and_fusion.2, bf16[512,8,64]{0,2,1:T(8,128)(2,1)S(1)} %bitcast.116, bf16[128,8,64]{0,2,1:T(8,128)(2,1)S(1)} %get-tuple-element.292), kind=kOutput, calls=%fused_computation.39.clone.1 | convolution fusion | flops 72875008 | bytes 4935680 | tf_op jit(solution)/shard_map/while/body/eval_jaxpr/qhd,khd->hqk/dot_general | solution.py:42
  113.1 5.0 %fusion.94 = f32[8,128,4,128]{1,0,3,2:T(8,128)S(1)} fusion(f32[8,128,4,128]{1,3,2,0:T(8,128)S(1)} %bitcast.114), kind=kOutput, calls=%fused_computation.23.clone.1 | output fusion | flops 66584576 | bytes 4194304 | tf_op jit(solution)/shard_map/reduce-window.6
  118.1 0.1 broadcast_add_fusion.2
  118.3 1.7 copy.38
  120.0 4.8 %fusion.97 = bf16[8,128,512]{1,2,0:T(8,128)(2,1)S(1)} fusion(f32[8,128,4,128]{1,3,2,0:T(8,128)} %copy.38, f32[8,512,128]{2,1,0:T(8,128)} %get-tuple-element.259, f32[8,128]{1,0:T(8,128)S(1)} %get-tuple-element.261, f32[8,512]{1,0:T(8,128)S(1)} %dynamic-slice_convert_fusion.2, pred[128,512]{0,1:T(8,128)(4,1)S(1)} %compare_and_fusion.2), kind=kLoop, calls=%fused_computation.12.clone.1 | loop fusion | flops 12058624 | bytes 5328896 | tf_op jit(solution)/shard_map/while/body/eval_jaxpr/convert_element_type | solution.py:55
  124.8 0.3 fusion.98
  125.2 2.9 %convolution_convert_fusion.1 = bf16[128,2048]{1,0:T(8,128)(2,1)} fusion(bf16[128,512]{0,1:T(8,128)(2,1)S(1)} %bitcast.118, bf16[512,2048]{1,0:T(8,128)(2,1)} %param.23), kind=kOutput, calls=%fused_computation.41 | convolution fusion | flops 268697600 | bytes 2752512 | tf_op jit(solution)/shard_map/dot_general | solution.py:113
  128.1 0.0 all-gather.8.cloned.1.call-start
  128.1 0.2 slice_reduce_fusion
  128.3 0.1 eq.25
  128.5 0.1 copy.28
  128.6 0.1 mul.162
  128.8 0.1 fusion.58
  128.9 1.4 scatter_custom_fusion
  130.3 2.2 scatter_custom_fusion.1
  132.5 0.1 mul.164
  132.6 0.8 dynamic_slice.28
  133.3 15.6 %reduce-scatter.3.cloned.1.call-done = bf16[128,512]{1,0:T(8,128)(2,1)} async-done(((bf16[128,2048]{1,0:T(8,128)(2,1)}), bf16[128,512]{1,0:T(8,128)(2,1)}) %reduce-scatter.3.cloned.1.call-update) | async-done | bytes 131088 | tf_op jit(solution)/shard_map/reduce_scatter | solution.py:133
  148.9 1.1 fusion.53
  150.0 5.8 %psum.7 = f32[128]{0:T(128)S(1)} all-reduce(f32[128]{0:T(128)S(1)} %get-tuple-element.193), channel_id=1, replica_groups=mesh['sp'=8,'tp'=4] {'tp'}, use_global_device_ids=true, to_apply=%region_9.10 | all-reduce | flops 128 | bytes 1024 | tf_op jit(solution)/shard_map/psum | solution.py:140
  155.8 0.1 fusion.55
  155.9 2.0 gather_fusion
  157.9 0.1 broadcast_multiply_fusion
  158.0 16.3 %all_to_all.10 = bf16[8,40,512]{2,1,0:T(8,128)(2,1)} all-to-all(bf16[8,40,512]{2,1,0:T(8,128)(2,1)S(1)} %broadcast_multiply_fusion), channel_id=1, replica_groups=mesh['sp'=8,'tp'=4] {'sp'}, dimensions={0} | all-to-all | bytes 655360 | tf_op jit(solution)/shard_map/all_to_all | solution.py:147
  174.3 0.0 all-gather.8.cloned.1.call-update
  174.4 0.2 reduce-scatter.5.cloned.1.call-start
  174.6 15.6 %all-gather.8.cloned.1.call-done = bf16[8,40,2048]{2,1,0:T(8,128)(2,1)} async-done(((bf16[8,40,512]{2,1,0:T(8,128)(2,1)}), bf16[8,40,2048]{2,1,0:T(8,128)(2,1)}) %all-gather.8.cloned.1.call-update) | async-done | bytes 1310736 | tf_op jit(solution)/shard_map/all_gather | solution.py:146
  190.1 2.8 %fusion.33 = f32[8,40,512]{2,1,0:T(8,128)S(1)} fusion(bf16[8,40,2048]{2,1,0:T(8,128)(2,1)} %all-gather.8.cloned.1.call-done, bf16[1,2048,512]{2,1,0:T(8,128)(2,1)} %param.27), kind=kOutput, calls=%fused_computation.50 | convolution fusion | flops 671252480 | bytes 4063232 | tf_op jit(solution)/shard_map/scd,df->scf/dot_general | solution.py:152
  193.0 4.8 %convolution_convert_fusion = bf16[8,40,2048]{2,1,0:T(8,128)(2,1)} fusion(bf16[1,512,2048]{2,1,0:T(8,128)(2,1)S(1)} %copy-done, bf16[8,40,2048]{2,1,0:T(8,128)(2,1)} %all-gather.8.cloned.1.call-done, bf16[1,2048,512]{2,1,0:T(8,128)(2,1)} %param.28, f32[8,40,512]{2,1,0:T(8,128)S(1)} %fusion.33), kind=kOutput, calls=%fused_computation.40 | convolution fusion | flops 1344307200 | bytes 7471104 | tf_op jit(solution)/shard_map/scf,fd->scd/dot_general | solution.py:155
  197.8 26.6 %reduce-scatter.5.cloned.1.call-done = bf16[8,40,512]{2,1,0:T(8,128)(2,1)} async-done(((bf16[8,40,2048]{2,1,0:T(8,128)(2,1)}), bf16[8,40,512]{2,1,0:T(8,128)(2,1)}) %reduce-scatter.5.cloned.1.call-update) | async-done | bytes 327696 | tf_op jit(solution)/shard_map/reduce_scatter | solution.py:156
  224.4 5.5 %all-to-all-start.1 = ((bf16[8,40,512]{2,1,0:T(8,128)(2,1)}), bf16[8,40,512]{2,1,0:T(8,128)(2,1)S(1)}, u32[]{:S(2)}, u32[]{:S(2)}) async-start(bf16[8,40,512]{2,1,0:T(8,128)(2,1)} %reduce-scatter.5.cloned.1.call-done), calls=%async_computation.3 | async-start | bytes 655360 | tf_op jit(solution)/shard_map/all_to_all | solution.py:157
  229.9 0.1 copy.31
  230.0 10.0 %all-to-all-done.1 = bf16[8,40,512]{2,1,0:T(8,128)(2,1)S(1)} async-done(((bf16[8,40,512]{2,1,0:T(8,128)(2,1)}), bf16[8,40,512]{2,1,0:T(8,128)(2,1)S(1)}, u32[]{:S(2)}, u32[]{:S(2)}) %all-to-all-start.1) | async-done | bytes 327712 | tf_op jit(solution)/shard_map/all_to_all | solution.py:157
  240.1 1.2 gather_fusion.1
  241.2 0.3 reshape.188
  241.5 0.7 multiply_reduce_fusion
  242.3 0.7 fusion.56
  (42 shorter events, 0.3 us)
Async XLA Ops:
  6.5 186.5 %copy-start = (bf16[1,512,2048]{2,1,0:T(8,128)(2,1)S(1)}, bf16[1,512,2048]{2,1,0:T(8,128)(2,1)}, u32[]{:S(2)}) copy-start(bf16[1,512,2048]{2,1,0:T(8,128)(2,1)} %param.29) | copy-start | bytes 6291460
  6.5 45.1 %all-gather.6.cloned.1.call-start = ((), (), s32[]{:S(2)}) async-start(), calls=%async_computation.5 | async-start | bytes 1179648 | tf_op jit(solution)/shard_map/all_gather | solution.py:91
  9.3 82.6 %all-gather.4.cloned.1.call-start = ((), (), s32[]{:S(2)}) async-start(), calls=%async_computation.4 | async-start | bytes 1179648 | tf_op jit(solution)/shard_map/all_gather | solution.py:92
  11.1 137.9 %reduce-scatter.3.cloned.1.call-start = ((), (), s32[]{:S(2)}) async-start(), calls=%async_computation.6 | async-start | bytes 655360 | tf_op jit(solution)/shard_map/reduce_scatter | solution.py:133
  125.1 3.4 %copy-start.1 = (s32[128,2]{0,1:T(2,128)S(1)}, s32[128,2]{0,1:T(2,128)}, u32[]{:S(2)}) copy-start(s32[128,2]{0,1:T(2,128)} %param.25) | copy-start | bytes 3076
  128.1 62.1 %all-gather.8.cloned.1.call-start = ((), (), s32[]{:S(2)}) async-start(), calls=%async_computation.7 | async-start | bytes 1638400 | tf_op jit(solution)/shard_map/all_gather | solution.py:146
  174.4 50.0 %reduce-scatter.5.cloned.1.call-start = ((), (), s32[]{:S(2)}) async-start(), calls=%async_computation.8 | async-start | bytes 1638400 | tf_op jit(solution)/shard_map/reduce_scatter | solution.py:156
  193.0 36.9 %copy-start.2 = (f32[128,2]{0,1:T(2,128)S(1)}, f32[128,2]{0,1:T(2,128)}, u32[]{:S(2)}) copy-start(f32[128,2]{0,1:T(2,128)} %param.26) | copy-start | bytes 3076
  224.4 15.7 %all-to-all-start.1 = ((bf16[8,40,512]{2,1,0:T(8,128)(2,1)}), bf16[8,40,512]{2,1,0:T(8,128)(2,1)S(1)}, u32[]{:S(2)}, u32[]{:S(2)}) async-start(bf16[8,40,512]{2,1,0:T(8,128)(2,1)} %reduce-scatter.5.cloned.1.call-done), calls=%async_computation.3 | async-start | bytes 655360 | tf_op jit(solution)/shard_map/all_to_all | solution.py:157
Sparse Core Ops, SparseCore 0:
  9.4 42.1 all-gather.5
  53.6 38.1 all-gather.3
  128.2 20.6 reduce-scatter.2
  174.5 15.6 all-gather.7
  197.9 26.4 reduce-scatter.4
where the time goes:
time: 250 us; the launch traced here: 249 us
  waiting for transfers between devices  117 us (47%)
  blocking collectives  50.3 us (20%)
  other arithmetic  25.5 us (10%)
  local copies, waits for them, and re-layouts  20.1 us (8%)
  matrix products  17.2 us (7%)
  between operations  13.4 us (5%)
  starting transfers between devices  5.86 us (2%)
    all_gather x1, waiting for transfers between devices, per_device(): lax.all_gather(values, 'sp', axis=0, tiled=True)  40.3 us
    all_gather x1, blocking collectives, per_device(): lax.all_gather(stick_bias, 'sp', axis=1, tiled=True)  28.2 us
    reduce_scatter x1, waiting for transfers between devices, per_device(): lax.psum_scatter(share.astype(jnp.bfloat16), 'tp', scatter_dimension=2, t...  26.6 us
    all_to_all x1, blocking collectives, per_device(): lax.all_to_all(outgoing, 'sp', split_axis=0, concat_axis=0, tiled=True)  16.3 us
    reduce_scatter x1, waiting for transfers between devices, per_device(): lax.psum_scatter(partial_value.astype(jnp.bfloat16), 'tp', scatter_dimens...  15.6 us
    all_gather x1, waiting for transfers between devices, per_device(): lax.all_gather(lax.all_to_all(outgoing, 'sp', split_axis=0, concat_axis=0...  15.6 us
    another operation x6, other arithmetic  10.7 us
    all_to_all x1, waiting for transfers between devices, per_device(): lax.all_to_all(returned, 'sp', split_axis=0, concat_axis=0, tiled=True)  10 us
  transfers between devices with their start and end apart: 6, of which 6 were waited for; matrix products, arithmetic and copies ran while one was open for 4% of the time, Pallas kernels for 0%

commit v1 on v0

--- a/solution.py
+++ b/solution.py
@@ -143,11 +143,11 @@
         own_cols * lax.rsqrt(square_total / model_width + epsilon)[:, None] * gain_cols
     ).astype(jnp.bfloat16)
     outgoing = (normed_share[source] * filled[:, None]).reshape(expert_count, capacity, -1)
-    piece = lax.all_gather(
-        lax.all_to_all(outgoing, "sp", split_axis=0, concat_axis=0, tiled=True),
-        "tp",
+    piece = jnp.concatenate(
+        lax.all_gather(
+            lax.all_to_all(outgoing, "sp", split_axis=0, concat_axis=0, tiled=True), "tp"
+        ),
         axis=2,
-        tiled=True,
     )
     gate_pre = jnp.einsum("scd,df->scf", piece, gate_local, preferred_element_type=jnp.float32)
     up_pre = jnp.einsum("scd,df->scf", piece, up_local, preferred_element_type=jnp.float32)

time: 250 us -> 251 us (level)
  no operation moved by 1% of the time
where the time goes in v1:
time: 251 us; the launch traced here: 250 us
  waiting for transfers between devices  117 us (47%)
  blocking collectives  50.3 us (20%)
  other arithmetic  25.5 us (10%)
  local copies, waits for them, and re-layouts  22 us (9%)
  matrix products  15.8 us (6%)
  between operations  13.4 us (5%)
  starting transfers between devices  5.86 us (2%)
    all_gather x1, waiting for transfers between devices, per_device(): lax.all_gather(values, 'sp', axis=0, tiled=True)  40.3 us
    all_gather x1, blocking collectives, per_device(): lax.all_gather(stick_bias, 'sp', axis=1, tiled=True)  28.2 us
    reduce_scatter x1, waiting for transfers between devices, per_device(): lax.psum_scatter(share.astype(jnp.bfloat16), 'tp', scatter_dimension=2, t...  26.5 us
    all_to_all x1, blocking collectives, per_device(): lax.all_to_all(outgoing, 'sp', split_axis=0, concat_axis=0, tiled=True)  16.3 us
    reduce_scatter x1, waiting for transfers between devices, per_device(): lax.psum_scatter(partial_value.astype(jnp.bfloat16), 'tp', scatter_dimens...  15.6 us
    all_gather x1, waiting for transfers between devices, per_device(): lax.all_gather(lax.all_to_all(outgoing, 'sp', split_axis=0, concat_axis=0...  15.6 us
    another operation x6, other arithmetic  10.7 us
    all_to_all x1, waiting for transfers between devices, per_device(): lax.all_to_all(returned, 'sp', split_axis=0, concat_axis=0, tiled=True)  10 us
  transfers between devices with their start and end apart: 6, of which 6 were waited for; matrix products, arithmetic and copies ran while one was open for 4% of the time, Pallas kernels for 0%

profile of v1, /device:TPU:0, one launch (start us, length us, event | category | flops | bytes accessed | tf_op | source)
XLA Modules:
  0.0 250.0 jit_solution(13687845225394225698)
XLA Ops:
  6.5 1.2 copy.37
  7.8 0.7 mul.146
  8.4 0.1 mul.147
  8.5 0.8 fusion.52
  9.3 0.0 all-gather.5.cloned.1.call-start
  9.4 1.7 copy.36
  11.1 0.0 reduce-scatter.3.cloned.1.call-start
  11.1 1.0 copy.38
  12.1 0.8 copy.40
  12.9 0.1 eq.29
  13.1 0.6 reduce-window.24
  13.7 28.2 %all_gather.17 = bf16[8,1024]{1,0:T(8,128)(2,1)S(1)} all-gather(bf16[8,128]{1,0:T(8,128)(2,1)} %param.20), channel_id=1, replica_groups=mesh['sp'=8,'tp'=4] {'sp'}, dimensions={1}, use_global_device_ids=true | all-gather | bytes 18432 | tf_op jit(solution)/shard_map/all_gather | solution.py:93
  42.0 0.7 multiply_convert_fusion
  42.7 8.9 %all-gather.7.cloned.1.call-done = bf16[1024,512]{0,1:T(8,128)(2,1)} async-done(((bf16[128,512]{0,1:T(8,128)(2,1)}), bf16[1024,512]{0,1:T(8,128)(2,1)}) %all-gather.7.cloned.1.call-update) | async-done | bytes 1048592 | tf_op jit(solution)/shard_map/all_gather | solution.py:91
  51.6 40.3 %all-gather.5.cloned.1.call-done = bf16[1024,512]{0,1:T(8,128)(2,1)} async-done(((bf16[128,512]{0,1:T(8,128)(2,1)}), bf16[1024,512]{0,1:T(8,128)(2,1)}) %all-gather.5.cloned.1.call-update) | async-done | bytes 1048592 | tf_op jit(solution)/shard_map/all_gather | solution.py:92
  91.9 33.3 %while.16 = (s32[]{:T(128)}, f32[128,8,64]{0,2,1:T(8,128)S(1)}, f32[8,128]{1,0:T(8,128)S(1)}, bf16[1024,512]{0,1:T(8,128)(2,1)}, bf16[1024,512]{0,1:T(8,128)(2,1...) while((s32[]{:T(128)}, f32[128,8,64]{0,2,1:T(8,128)S(1)}, ...), condition=%wide.region_6.7_spmd.clone, body=%wide.region_2.6_spmd.clone.sunk | while | flops 219436672 | bytes 27240652 | solution.py:111
  91.9 1.3 constant_dynamic-slice_fusion.3
  93.2 0.2 compare_and_fusion.2
  93.4 3.0 %fusion.93 = (f32[8,128]{1,0:T(8,128)S(1)}, f32[8,128,512]{1,2,0:T(8,128)S(1)}, f32[8,512,128]{2,1,0:T(8,128)}) fusion(f32[8,512]{1,0:T(8,128)S(1)} %dynamic-slice_convert_fusion.2, pred[128,512]{0,1:T(8,128)(4,1)S(1)} %compare_and_fusion.2, bf16[512,8,64]{0,2,1:T(8,128)(2,1)S(1)} %bitcast.121, bf16[128,8,64]{0,2,1:T(8,128)(2,1)S(1)} %get-tuple-element.292), kind=kOutput, calls=%fused_computation.39.clone.1 | convolution fusion | flops 72875008 | bytes 4935680 | tf_op jit(solution)/shard_map/while/body/eval_jaxpr/qhd,khd->hqk/dot_general | solution.py:42
  96.4 5.0 %fusion.94 = f32[8,128,4,128]{1,0,3,2:T(8,128)S(1)} fusion(f32[8,128,4,128]{1,3,2,0:T(8,128)S(1)} %bitcast.119), kind=kOutput, calls=%fused_computation.23.clone.1 | output fusion | flops 66584576 | bytes 4194304 | tf_op jit(solution)/shard_map/reduce-window.6
  101.5 0.1 broadcast_add_fusion.2
  101.6 1.7 copy.51
  103.3 4.8 %fusion.97 = bf16[8,128,512]{1,2,0:T(8,128)(2,1)S(1)} fusion(f32[8,128,4,128]{1,3,2,0:T(8,128)} %copy.51, f32[8,512,128]{2,1,0:T(8,128)} %get-tuple-element.259, f32[8,128]{1,0:T(8,128)S(1)} %get-tuple-element.261, f32[8,512]{1,0:T(8,128)S(1)} %dynamic-slice_convert_fusion.2, pred[128,512]{0,1:T(8,128)(4,1)S(1)} %compare_and_fusion.2), kind=kLoop, calls=%fused_computation.12.clone.1 | loop fusion | flops 12058624 | bytes 5328896 | tf_op jit(solution)/shard_map/while/body/eval_jaxpr/convert_element_type | solution.py:55
  108.1 0.3 fusion.98
  108.5 1.3 constant_dynamic-slice_fusion.3
  109.8 0.2 compare_and_fusion.2
  110.1 3.0 %fusion.93 = (f32[8,128]{1,0:T(8,128)S(1)}, f32[8,128,512]{1,2,0:T(8,128)S(1)}, f32[8,512,128]{2,1,0:T(8,128)}) fusion(f32[8,512]{1,0:T(8,128)S(1)} %dynamic-slice_convert_fusion.2, pred[128,512]{0,1:T(8,128)(4,1)S(1)} %compare_and_fusion.2, bf16[512,8,64]{0,2,1:T(8,128)(2,1)S(1)} %bitcast.121, bf16[128,8,64]{0,2,1:T(8,128)(2,1)S(1)} %get-tuple-element.292), kind=kOutput, calls=%fused_computation.39.clone.1 | convolution fusion | flops 72875008 | bytes 4935680 | tf_op jit(solution)/shard_map/while/body/eval_jaxpr/qhd,khd->hqk/dot_general | solution.py:42
  113.1 5.0 %fusion.94 = f32[8,128,4,128]{1,0,3,2:T(8,128)S(1)} fusion(f32[8,128,4,128]{1,3,2,0:T(8,128)S(1)} %bitcast.119), kind=kOutput, calls=%fused_computation.23.clone.1 | output fusion | flops 66584576 | bytes 4194304 | tf_op jit(solution)/shard_map/reduce-window.6
  118.1 0.1 broadcast_add_fusion.2
  118.3 1.7 copy.51
  120.0 4.8 %fusion.97 = bf16[8,128,512]{1,2,0:T(8,128)(2,1)S(1)} fusion(f32[8,128,4,128]{1,3,2,0:T(8,128)} %copy.51, f32[8,512,128]{2,1,0:T(8,128)} %get-tuple-element.259, f32[8,128]{1,0:T(8,128)S(1)} %get-tuple-element.261, f32[8,512]{1,0:T(8,128)S(1)} %dynamic-slice_convert_fusion.2, pred[128,512]{0,1:T(8,128)(4,1)S(1)} %compare_and_fusion.2), kind=kLoop, calls=%fused_computation.12.clone.1 | loop fusion | flops 12058624 | bytes 5328896 | tf_op jit(solution)/shard_map/while/body/eval_jaxpr/convert_element_type | solution.py:55
  124.8 0.3 fusion.98
  125.2 2.9 %convolution_convert_fusion.1 = bf16[128,2048]{1,0:T(8,128)(2,1)} fusion(bf16[128,512]{0,1:T(8,128)(2,1)S(1)} %bitcast.126, bf16[512,2048]{1,0:T(8,128)(2,1)} %param.23), kind=kOutput, calls=%fused_computation.41 | convolution fusion | flops 268697600 | bytes 2752512 | tf_op jit(solution)/shard_map/dot_general | solution.py:113
  128.1 0.0 all-gather.9.cloned.1.call-start
  128.1 0.2 slice_reduce_fusion
  128.3 0.1 eq.25
  128.5 0.1 copy.39
  128.6 0.1 mul.162
  128.8 0.1 fusion.58
  128.9 1.4 scatter_custom_fusion
  130.3 2.2 scatter_custom_fusion.1
  132.5 0.1 mul.164
  132.6 0.8 dynamic_slice.28
  133.3 15.6 %reduce-scatter.3.cloned.1.call-done = bf16[128,512]{1,0:T(8,128)(2,1)} async-done(((bf16[128,2048]{1,0:T(8,128)(2,1)}), bf16[128,512]{1,0:T(8,128)(2,1)}) %reduce-scatter.3.cloned.1.call-update) | async-done | bytes 131088 | tf_op jit(solution)/shard_map/reduce_scatter | solution.py:133
  148.9 1.1 fusion.53
  150.0 5.8 %psum.7 = f32[128]{0:T(128)S(1)} all-reduce(f32[128]{0:T(128)S(1)} %get-tuple-element.193), channel_id=1, replica_groups=mesh['sp'=8,'tp'=4] {'tp'}, use_global_device_ids=true, to_apply=%region_9.10 | all-reduce | flops 128 | bytes 1024 | tf_op jit(solution)/shard_map/psum | solution.py:140
  155.8 0.1 fusion.55
  155.9 2.0 gather_fusion
  157.9 0.1 broadcast_multiply_fusion
  158.0 16.3 %all_to_all.10 = bf16[8,40,512]{2,1,0:T(8,128)(2,1)} all-to-all(bf16[8,40,512]{2,1,0:T(8,128)(2,1)S(1)} %broadcast_multiply_fusion), channel_id=1, replica_groups=mesh['sp'=8,'tp'=4] {'sp'}, dimensions={0} | all-to-all | bytes 655360 | tf_op jit(solution)/shard_map/all_to_all | solution.py:148
  174.4 0.2 reduce-scatter.5.cloned.1.call-start
  174.6 15.6 %all-gather.9.cloned.1.call-done = bf16[32,40,512]{2,1,0:T(8,128)(2,1)} async-done(((bf16[8,40,512]{2,1,0:T(8,128)(2,1)}), bf16[32,40,512]{2,1,0:T(8,128)(2,1)}) %all-gather.9.cloned.1.call-update) | async-done | bytes 1310736 | tf_op jit(solution)/shard_map/all_gather | solution.py:147
  190.1 1.6 copy.45
  191.8 0.3 copy-done.3
  192.1 1.8 fusion.33
  193.9 4.5 %convolution_convert_fusion = bf16[8,40,2048]{2,1,0:T(8,128)(2,1)} fusion(bf16[1,512,2048]{2,1,0:T(8,128)(2,1)S(1)} %copy-done, bf16[8,40,2048]{2,1,0:T(8,128)(2,1)S(1)} %bitcast.125, bf16[1,2048,512]{2,1,0:T(8,128)(2,1)} %param.28, f32[8,40,512]{2,1,0:T(8,128)} %fusion.33), kind=kOutput, calls=%fused_computation.40 | convolution fusion | flops 1344307200 | bytes 7471104 | tf_op jit(solution)/shard_map/scf,fd->scd/dot_general | solution.py:155
  198.4 26.5 %reduce-scatter.5.cloned.1.call-done = bf16[8,40,512]{2,1,0:T(8,128)(2,1)} async-done(((bf16[8,40,2048]{2,1,0:T(8,128)(2,1)}), bf16[8,40,512]{2,1,0:T(8,128)(2,1)}) %reduce-scatter.5.cloned.1.call-update) | async-done | bytes 327696 | tf_op jit(solution)/shard_map/reduce_scatter | solution.py:156
  224.9 5.5 %all-to-all-start.1 = ((bf16[8,40,512]{2,1,0:T(8,128)(2,1)}), bf16[8,40,512]{2,1,0:T(8,128)(2,1)S(1)}, u32[]{:S(2)}, u32[]{:S(2)}) async-start(bf16[8,40,512]{2,1,0:T(8,128)(2,1)} %reduce-scatter.5.cloned.1.call-done), calls=%async_computation.3 | async-start | bytes 655360 | tf_op jit(solution)/shard_map/all_to_all | solution.py:157
  230.4 0.1 copy.43
  230.6 10.0 %all-to-all-done.1 = bf16[8,40,512]{2,1,0:T(8,128)(2,1)S(1)} async-done(((bf16[8,40,512]{2,1,0:T(8,128)(2,1)}), bf16[8,40,512]{2,1,0:T(8,128)(2,1)S(1)}, u32[]{:S(2)}, u32[]{:S(2)}) %all-to-all-start.1) | async-done | bytes 327712 | tf_op jit(solution)/shard_map/all_to_all | solution.py:157
  240.6 1.2 gather_fusion.1
  241.7 0.3 reshape.196
  242.1 0.7 multiply_reduce_fusion
  242.8 0.7 fusion.56
  (45 shorter events, 0.4 us)
Async XLA Ops:
  6.5 187.3 %copy-start = (bf16[1,512,2048]{2,1,0:T(8,128)(2,1)S(1)}, bf16[1,512,2048]{2,1,0:T(8,128)(2,1)}, u32[]{:S(2)}) copy-start(bf16[1,512,2048]{2,1,0:T(8,128)(2,1)} %param.29) | copy-start | bytes 6291460
  6.5 45.1 %all-gather.7.cloned.1.call-start = ((), (), s32[]{:S(2)}) async-start(), calls=%async_computation.5 | async-start | bytes 1179648 | tf_op jit(solution)/shard_map/all_gather | solution.py:91
  9.3 82.6 %all-gather.5.cloned.1.call-start = ((), (), s32[]{:S(2)}) async-start(), calls=%async_computation.4 | async-start | bytes 1179648 | tf_op jit(solution)/shard_map/all_gather | solution.py:92
  11.1 137.9 %reduce-scatter.3.cloned.1.call-start = ((), (), s32[]{:S(2)}) async-start(), calls=%async_computation.6 | async-start | bytes 655360 | tf_op jit(solution)/shard_map/reduce_scatter | solution.py:133
  125.1 3.4 %copy-start.1 = (s32[128,2]{0,1:T(2,128)S(1)}, s32[128,2]{0,1:T(2,128)}, u32[]{:S(2)}) copy-start(s32[128,2]{0,1:T(2,128)} %param.25) | copy-start | bytes 3076
  128.1 62.1 %all-gather.9.cloned.1.call-start = ((), (), s32[]{:S(2)}) async-start(), calls=%async_computation.8 | async-start | bytes 1638400 | tf_op jit(solution)/shard_map/all_gather | solution.py:147
  174.4 50.6 %reduce-scatter.5.cloned.1.call-start = ((), (), s32[]{:S(2)}) async-start(), calls=%async_computation.7 | async-start | bytes 1638400 | tf_op jit(solution)/shard_map/reduce_scatter | solution.py:156
  190.1 2.0 copy-start.3
  193.9 36.5 %copy-start.2 = (f32[128,2]{0,1:T(2,128)S(1)}, f32[128,2]{0,1:T(2,128)}, u32[]{:S(2)}) copy-start(f32[128,2]{0,1:T(2,128)} %param.26) | copy-start | bytes 3076
  224.9 15.7 %all-to-all-start.1 = ((bf16[8,40,512]{2,1,0:T(8,128)(2,1)}), bf16[8,40,512]{2,1,0:T(8,128)(2,1)S(1)}, u32[]{:S(2)}, u32[]{:S(2)}) async-start(bf16[8,40,512]{2,1,0:T(8,128)(2,1)} %reduce-scatter.5.cloned.1.call-done), calls=%async_computation.3 | async-start | bytes 655360 | tf_op jit(solution)/shard_map/all_to_all | solution.py:157
Sparse Core Ops, SparseCore 0:
  9.4 42.1 all-gather.6
  53.6 38.1 all-gather.4
  128.2 20.6 reduce-scatter.2
  174.5 15.6 all-gather.8
  198.5 26.3 reduce-scatter.4
